TPU v7x, 32 devices: a whole 2x2x4 slice. The times are simulated.
32 devices in a mesh: ra: 16 (over z, y, x), cb: 2 (over core).
Axes of the slice: x: 2, y: 2, z: 4, core: 2. Of those that a mesh axis runs over, the one named last changes fastest.
Arguments:
- activations: bfloat16 [768, 4096], P('ra', 'cb'), may hold values from -230 to 230
- gain_first: float32 [4096], P('cb'), may hold values from 0.1 to 1.9
- gate_weight: float32 [11264, 4096], P('ra', 'cb'), may hold values from -0.125 to 0.125
- gate_scale: float32 [11264], P('ra'), may hold values from 0.5 to 2
- up_weight: float32 [11264, 4096], P('ra', 'cb'), may hold values from -0.125 to 0.125
- up_scale: float32 [11264], P('ra'), may hold values from 0.5 to 2
- down_weight: float32 [11264, 4096], P('ra', 'cb'), may hold values from -0.0546875 to 0.0546875
- down_scale: float32 [4096], P('cb'), may hold values from 0.35 to 2.8
- gain_second: float32 [4096], P('cb'), may hold values from 0.1 to 1.9
Outputs:
- normed: bfloat16 [768, 4096], P('ra', 'cb')
All inputs are finite; a program needn't handle non-finite values.
Results may differ from a plain program's by a relative error of at most 0.011.
Values may be sent and summed in bfloat16 or wider, within the bound.
A program may use at most 64 MiB of HBM per device.

v0:
```python
import jax
import jax.numpy as jnp
from jax import lax
from jax.sharding import PartitionSpec as P

EPS = 1e-06


def per_device(
    activations,
    gain_first,
    gate_weight,
    gate_scale,
    up_weight,
    up_scale,
    down_weight,
    down_scale,
    gain_second,
):
    inputs = activations.astype(jnp.float32)
    features = activations.shape[1] * lax.axis_size("cb")
    gate_local = gate_weight.astype(jnp.bfloat16)
    up_local = up_weight.astype(jnp.bfloat16)
    down_local = down_weight.astype(jnp.bfloat16)
    gathered = lax.all_gather(activations, "ra", axis=0, tiled=True)
    wide_rows = gathered.astype(jnp.float32)
    row_squares = jnp.sum(wide_rows * wide_rows, axis=1)
    scaled = (wide_rows * gain_first).astype(jnp.bfloat16)
    contract = (((1,), (1,)), ((), ()))
    squares = lax.psum(row_squares, "cb")
    gate_part = lax.dot_general(gate_local, scaled, contract, preferred_element_type=jnp.float32)
    up_part = lax.dot_general(up_local, scaled, contract, preferred_element_type=jnp.float32)
    gate_sum, up_sum = lax.psum((gate_part, up_part), "cb")
    rscale_first = lax.rsqrt(squares / features + EPS)[None, :]
    gate_full = gate_sum * rscale_first * gate_scale[:, None]
    up_full = up_sum * rscale_first * up_scale[:, None]
    hidden = (jax.nn.silu(gate_full) * up_full).astype(jnp.bfloat16)
    summed = lax.psum_scatter(
        lax.dot_general(
            hidden, down_local, (((0,), (0,)), ((), ())), preferred_element_type=jnp.float32
        ),
        "ra",
        scatter_dimension=0,
        tiled=True,
    )
    stream = 0.1 * inputs + summed * down_scale
    second = lax.psum(jnp.sum(stream * stream, axis=1), "cb")
    rscale_second = lax.rsqrt(second / features + EPS)[:, None]
    return (stream * rscale_second * gain_second).astype(jnp.bfloat16)


def solution(mesh):
    placed = (
        P("ra", "cb"),
        P("cb"),
        P("ra", "cb"),
        P("ra"),
        P("ra", "cb"),
        P("ra"),
        P("ra", "cb"),
        P("cb"),
        P("cb"),
    )
    return jax.shard_map(
        per_device, mesh=mesh, in_specs=placed, out_specs=P("ra", "cb"), check_vma=False
    )
```

profile of v0, /device:TPU:0, one launch (start us, length us, event | category | flops | bytes accessed | tf_op | source)
XLA Modules:
  0.0 292.0 jit_solution(9927717845892913069)
XLA Ops:
  6.5 0.0 all-gather.2.cloned.1.call-start
  6.5 0.7 all-gather.2.cloned.1.call-update
  7.3 0.0 copy-start.4
  7.3 0.0 all-reduce.3.cloned.1.call-start
  7.3 73.4 %all-gather.2.cloned.1.call-done = bf16[768,2048]{1,0:T(8,128)(2,1)} async-done(((bf16[48,2048]{1,0:T(8,128)(2,1)}), bf16[768,2048]{1,0:T(8,128)(2,1)}) %all-gather.2.cloned.1.call-update) | async-done | bytes 3145744 | tf_op jit(solution)/shard_map/all_gather | solution.py:25
  80.7 7.5 %fusion.15 = f32[704,768]{1,0:T(8,128)} fusion(f32[704,2048]{1,0:T(8,128)} %param.13, bf16[768,2048]{1,0:T(8,128)(2,1)} %all-gather.2.cloned.1.call-done, f32[2048]{0:T(1024)} %param.10), kind=kOutput, calls=%fused_computation.12 | convolution fusion | flops 2220752896 | bytes 11083776 | tf_op jit(solution)/shard_map/dot_general | solution.py:32
  88.3 0.0 copy-done.4
  88.3 0.0 copy-done
  88.3 6.4 %fusion.10 = f32[704,768]{1,0:T(8,128)} fusion(f32[704,2048]{1,0:T(8,128)} %param.11, bf16[768,2048]{1,0:T(8,128)(2,1)S(1)} %copy-done, f32[2048]{0:T(1024)S(1)} %copy-done.4), kind=kOutput, calls=%fused_computation.11 | convolution fusion | flops 2220752896 | bytes 11083776 | tf_op jit(solution)/shard_map/dot_general | solution.py:31
  94.7 0.0 all-reduce.3.cloned.1.call-update
  94.7 0.0 reduce-scatter.2.cloned.1.call-start
  94.8 0.7 fusion.1
  95.5 2.5 psum.29
  97.9 23.9 %all-reduce.3.cloned.1.call-done = (f32[704,768]{1,0:T(8,128)}, f32[704,768]{1,0:T(8,128)}) async-done(((f32[704,768]{1,0:T(8,128)}, f32[704,768]{1,0:T(8,128)}), (f32[704,768]{1,0:T(8,128)}, f32[704,768]{1,0:T(8,128)})) %all-reduce.3.cloned.1.call-update) | async-done | bytes 4325392 | tf_op jit(solution)/shard_map/psum | solution.py:33
  121.9 0.0 copy-done.5
  121.9 0.0 copy-done.6
  121.9 9.5 %fusion.2 = f32[768,2048]{1,0:T(8,128)} fusion(f32[704,2048]{1,0:T(8,128)} %param.15, f32[704,768]{1,0:T(8,128)} %get-tuple-element.5, f32[704,768]{1,0:T(8,128)} %get-tuple-element.6, f32[704]{0:T(1024)S(1)} %copy-done.5, f32[704]{0:T(1024)S(1)} %copy-done.6, f32[768]{0:T(1024)S(1)} %add_rsqrt_fusion), kind=kOutput, calls=%fused_computation.4 | convolution fusion | flops 2221441024 | bytes 16392704 | tf_op jit(solution)/shard_map/dot_general | solution.py:39
  131.4 0.0 reduce-scatter.2.cloned.1.call-update
  131.4 148.7 %reduce-scatter.2.cloned.1.call-done = f32[48,2048]{1,0:T(8,128)} async-done(((f32[768,2048]{1,0:T(8,128)}), f32[48,2048]{1,0:T(8,128)}) %reduce-scatter.2.cloned.1.call-update) | async-done | bytes 393232 | tf_op jit(solution)/shard_map/reduce_scatter | solution.py:38
  280.1 0.0 copy-done.1
  280.1 0.0 copy-done.2
  280.1 1.2 multiply_reduce_fusion
  281.2 2.5 psum.31
  283.7 1.8 multiply_convert_fusion.2
  (9 shorter events, 0.0 us)
Async XLA Ops:
  6.5 74.2 %all-gather.2.cloned.1.call-start = ((), (), s32[]{:S(2)}) async-start(), calls=%async_computation.1 | async-start | bytes 3342336 | tf_op jit(solution)/shard_map/all_gather | solution.py:25
  7.3 81.0 %copy-start.4 = (f32[2048]{0:T(1024)S(1)}, f32[2048]{0:T(1024)}, u32[]{:S(2)}) copy-start(f32[2048]{0:T(1024)} %param.10) | copy-start | bytes 24580
  7.3 114.6 %all-reduce.3.cloned.1.call-start = ((), (), s32[]{:S(2)}) async-start(), calls=%async_computation.3 | async-start | bytes 8650752 | tf_op jit(solution)/shard_map/psum | solution.py:33
  80.7 7.6 %copy-start = (bf16[768,2048]{1,0:T(8,128)(2,1)S(1)}, bf16[768,2048]{1,0:T(8,128)(2,1)}, u32[]{:S(2)}) copy-start(bf16[768,2048]{1,0:T(8,128)(2,1)} %all-gather.2.cloned.1.call-done) | copy-start | bytes 9437188
  94.7 27.2 %copy-start.5 = (f32[704]{0:T(1024)S(1)}, f32[704]{0:T(1024)}, u32[]{:S(2)}) copy-start(f32[704]{0:T(1024)} %param.14) | copy-start | bytes 8452
  94.7 27.2 %copy-start.6 = (f32[704]{0:T(1024)S(1)}, f32[704]{0:T(1024)}, u32[]{:S(2)}) copy-start(f32[704]{0:T(1024)} %param.12) | copy-start | bytes 8452
  94.7 185.3 %reduce-scatter.2.cloned.1.call-start = ((), (), s32[]{:S(2)}) async-start(), calls=%async_computation.2 | async-start | bytes 6684672 | tf_op jit(solution)/shard_map/reduce_scatter | solution.py:38
  131.3 148.7 %copy-start.1 = (bf16[48,2048]{1,0:T(8,128)(2,1)S(1)}, bf16[48,2048]{1,0:T(8,128)(2,1)}, u32[]{:S(2)}) copy-start(bf16[48,2048]{1,0:T(8,128)(2,1)} %param.9) | copy-start | bytes 589828
  131.3 148.7 %copy-start.2 = (f32[2048]{0:T(1024)S(1)}, f32[2048]{0:T(1024)}, u32[]{:S(2)}) copy-start(f32[2048]{0:T(1024)} %param.16) | copy-start | bytes 24580
  131.4 152.4 %copy-start.3 = (f32[2048]{0:T(1024)S(1)}, f32[2048]{0:T(1024)}, u32[]{:S(2)}) copy-start(f32[2048]{0:T(1024)} %param.17) | copy-start | bytes 24580
Sparse Core Ops, SparseCore 0:
  10.1 70.5 all-gather.1
  94.9 26.9 all-reduce.2
  131.5 148.5 reduce-scatter.1
where the time goes:
time: 292 us
  waiting for transfers between devices  247 us (85%)
  matrix products  23.4 us (8%)
  between operations  13.1 us (4%)
  blocking collectives  4.95 us (2%)
  other arithmetic  3.66 us (1%)
    reduce_scatter x1, waiting for transfers between devices, per_device(): lax.psum_scatter(lax.dot_general(hidden, down_local, (((0,), (0,)), ((),...  149 us
    all_gather x1, waiting for transfers between devices, per_device(): gathered = lax.all_gather(activations, 'ra', axis=0, tiled=True)  73.4 us
    psum x1, waiting for transfers between devices, per_device(): gate_sum, up_sum = lax.psum((gate_part, up_part), 'cb')  23.9 us
    dot_general x1, matrix products, per_device(): lax.dot_general(hidden, down_local, (((0,), (0,)), ((), ())), preferred_e...  9.48 us
    dot_general x1, matrix products, per_device(): lax.dot_general(up_local, scaled, contract, preferred_element_type=jnp.fl...  7.55 us
    dot_general x1, matrix products, per_device(): lax.dot_general(gate_local, scaled, contract, preferred_element_type=jnp....  6.42 us
  transfers between devices with their start and end apart: 3, of which 3 were waited for; matrix products, arithmetic and copies ran while one was open for 0% of the time, Pallas kernels for 0%

commit v1 on v0

--- a/solution.py
+++ b/solution.py
@@ -22,7 +22,12 @@
     gate_local = gate_weight.astype(jnp.bfloat16)
     up_local = up_weight.astype(jnp.bfloat16)
     down_local = down_weight.astype(jnp.bfloat16)
-    gathered = lax.all_gather(activations, "ra", axis=0, tiled=True)
+    ring = [activations]
+    for hop in range(15):
+        ring.append(lax.ppermute(ring[-1], "ra", [(dev, (dev + 1) % 16) for dev in range(16)]))
+    gathered = jnp.roll(
+        jnp.concatenate(ring[::-1], axis=0), (lax.axis_index("ra") + 1) * ring[0].shape[0], axis=0
+    )
     wide_rows = gathered.astype(jnp.float32)
     row_squares = jnp.sum(wide_rows * wide_rows, axis=1)
     scaled = (wide_rows * gain_first).astype(jnp.bfloat16)

time: 292 us -> 359 us (1.23)
  waiting for transfers between devices: 247 us -> 310 us
  matrix products: 23.4 us -> 17.1 us
    ppermute x0 -> x15, waiting for transfers between devices: none -> 144 us  [per_device(): lax.ppermute(ring[-1], 'ra', [(dev, (dev + 1) % 16) for dev in range(16)])]
    all_gather x1 -> x0, waiting for transfers between devices: 73.4 us -> none  [per_device(): gathered = lax.all_gather(activations, 'ra', axis=0, tiled=True)]
    psum x1, waiting for transfers between devices: 23.9 us -> 18.7 us  [per_device(): gate_sum, up_sum = lax.psum((gate_part, up_part), 'cb')]
    dot_general x1, matrix products: 7.55 us -> 3.83 us  [per_device(): lax.dot_general(up_local, scaled, contract, preferred_element_type=jnp.fl...]
  transfers between devices with their start and end apart: 3 -> 17, of which waited for: 3 -> 17; matrix products, arithmetic and copies ran while one was open for 0% -> 1% of each run, Pallas kernels for 0% -> 0%
where the time goes in v1:
time: 359 us
  waiting for transfers between devices  310 us (86%)
  matrix products  17.1 us (5%)
  between operations  13.7 us (4%)
  other arithmetic  6.2 us (2%)
  blocking collectives  4.94 us (1%)
    reduce_scatter x1, waiting for transfers between devices, per_device(): lax.psum_scatter(lax.dot_general(hidden, down_local, (((0,), (0,)), ((),...  148 us
    ppermute x15, waiting for transfers between devices, per_device(): lax.ppermute(ring[-1], 'ra', [(dev, (dev + 1) % 16) for dev in range(16)])  144 us
    psum x1, waiting for transfers between devices, per_device(): gate_sum, up_sum = lax.psum((gate_part, up_part), 'cb')  18.7 us
    dot_general x1, matrix products, per_device(): lax.dot_general(hidden, down_local, (((0,), (0,)), ((), ())), preferred_e...  9.49 us
  transfers between devices with their start and end apart: 17, of which 17 were waited for; matrix products, arithmetic and copies ran while one was open for 1% of the time, Pallas kernels for 0%

profile of v1, /device:TPU:0, one launch (start us, length us, event | category | flops | bytes accessed | tf_op | source)
XLA Modules:
  0.0 358.7 jit_solution(11883989351126041309)
XLA Ops:
  6.5 3.0 collective-permute-start
  9.5 9.2 %collective-permute-done = bf16[48,2048]{1,0:T(8,128)(2,1)S(1)} collective-permute-done((bf16[48,2048]{1,0:T(8,128)(2,1)}, bf16[48,2048]{1,0:T(8,128)(2,1)S(1)}, u32[]{:S(2)}, u32[]{:S(2)}) %collective-permute-start) | collective-permute-done | bytes 196640 | tf_op jit(solution)/shard_map/ppermute | solution.py:27
  18.7 9.7 %collective-permute-done.1 = bf16[48,2048]{1,0:T(8,128)(2,1)S(1)} collective-permute-done((bf16[48,2048]{1,0:T(8,128)(2,1)S(1)}, bf16[48,2048]{1,0:T(8,128)(2,1)S(1)}, u32[]{:S(2)}, u32[]{:S(2)}) %collective-permute-start.1) | collective-permute-done | bytes 196640 | tf_op jit(solution)/shard_map/ppermute | solution.py:27
  28.3 9.3 %collective-permute-done.2 = bf16[48,2048]{1,0:T(8,128)(2,1)S(1)} collective-permute-done((bf16[48,2048]{1,0:T(8,128)(2,1)S(1)}, bf16[48,2048]{1,0:T(8,128)(2,1)S(1)}, u32[]{:S(2)}, u32[]{:S(2)}) %collective-permute-start.2) | collective-permute-done | bytes 196640 | tf_op jit(solution)/shard_map/ppermute | solution.py:27
  37.6 9.3 %collective-permute-done.3 = bf16[48,2048]{1,0:T(8,128)(2,1)S(1)} collective-permute-done((bf16[48,2048]{1,0:T(8,128)(2,1)S(1)}, bf16[48,2048]{1,0:T(8,128)(2,1)S(1)}, u32[]{:S(2)}, u32[]{:S(2)}) %collective-permute-start.3) | collective-permute-done | bytes 196640 | tf_op jit(solution)/shard_map/ppermute | solution.py:27
  46.9 9.3 %collective-permute-done.4 = bf16[48,2048]{1,0:T(8,128)(2,1)S(1)} collective-permute-done((bf16[48,2048]{1,0:T(8,128)(2,1)S(1)}, bf16[48,2048]{1,0:T(8,128)(2,1)S(1)}, u32[]{:S(2)}, u32[]{:S(2)}) %collective-permute-start.4) | collective-permute-done | bytes 196640 | tf_op jit(solution)/shard_map/ppermute | solution.py:27
  56.1 9.3 %collective-permute-done.5 = bf16[48,2048]{1,0:T(8,128)(2,1)S(1)} collective-permute-done((bf16[48,2048]{1,0:T(8,128)(2,1)S(1)}, bf16[48,2048]{1,0:T(8,128)(2,1)S(1)}, u32[]{:S(2)}, u32[]{:S(2)}) %collective-permute-start.5) | collective-permute-done | bytes 196640 | tf_op jit(solution)/shard_map/ppermute | solution.py:27
  65.4 10.4 %collective-permute-done.6 = bf16[48,2048]{1,0:T(8,128)(2,1)S(1)} collective-permute-done((bf16[48,2048]{1,0:T(8,128)(2,1)S(1)}, bf16[48,2048]{1,0:T(8,128)(2,1)S(1)}, u32[]{:S(2)}, u32[]{:S(2)}) %collective-permute-start.6) | collective-permute-done | bytes 196640 | tf_op jit(solution)/shard_map/ppermute | solution.py:27
  75.8 11.2 %collective-permute-done.7 = bf16[48,2048]{1,0:T(8,128)(2,1)S(1)} collective-permute-done((bf16[48,2048]{1,0:T(8,128)(2,1)S(1)}, bf16[48,2048]{1,0:T(8,128)(2,1)S(1)}, u32[]{:S(2)}, u32[]{:S(2)}) %collective-permute-start.7) | collective-permute-done | bytes 196640 | tf_op jit(solution)/shard_map/ppermute | solution.py:27
  87.0 10.3 %collective-permute-done.8 = bf16[48,2048]{1,0:T(8,128)(2,1)S(1)} collective-permute-done((bf16[48,2048]{1,0:T(8,128)(2,1)S(1)}, bf16[48,2048]{1,0:T(8,128)(2,1)S(1)}, u32[]{:S(2)}, u32[]{:S(2)}) %collective-permute-start.8) | collective-permute-done | bytes 196640 | tf_op jit(solution)/shard_map/ppermute | solution.py:27
  97.3 9.5 %collective-permute-done.9 = bf16[48,2048]{1,0:T(8,128)(2,1)S(1)} collective-permute-done((bf16[48,2048]{1,0:T(8,128)(2,1)S(1)}, bf16[48,2048]{1,0:T(8,128)(2,1)S(1)}, u32[]{:S(2)}, u32[]{:S(2)}) %collective-permute-start.9) | collective-permute-done | bytes 196640 | tf_op jit(solution)/shard_map/ppermute | solution.py:27
  106.8 9.3 %collective-permute-done.10 = bf16[48,2048]{1,0:T(8,128)(2,1)S(1)} collective-permute-done((bf16[48,2048]{1,0:T(8,128)(2,1)S(1)}, bf16[48,2048]{1,0:T(8,128)(2,1)S(1)}, u32[]{:S(2)}, u32[]{:S(2)}) %collective-permute-start.10) | collective-permute-done | bytes 196640 | tf_op jit(solution)/shard_map/ppermute | solution.py:27
  116.1 9.3 %collective-permute-done.11 = bf16[48,2048]{1,0:T(8,128)(2,1)S(1)} collective-permute-done((bf16[48,2048]{1,0:T(8,128)(2,1)S(1)}, bf16[48,2048]{1,0:T(8,128)(2,1)S(1)}, u32[]{:S(2)}, u32[]{:S(2)}) %collective-permute-start.11) | collective-permute-done | bytes 196640 | tf_op jit(solution)/shard_map/ppermute | solution.py:27
  125.3 9.3 %collective-permute-done.12 = bf16[48,2048]{1,0:T(8,128)(2,1)S(1)} collective-permute-done((bf16[48,2048]{1,0:T(8,128)(2,1)S(1)}, bf16[48,2048]{1,0:T(8,128)(2,1)S(1)}, u32[]{:S(2)}, u32[]{:S(2)}) %collective-permute-start.12) | collective-permute-done | bytes 196640 | tf_op jit(solution)/shard_map/ppermute | solution.py:27
  134.6 9.3 %collective-permute-done.13 = bf16[48,2048]{1,0:T(8,128)(2,1)S(1)} collective-permute-done((bf16[48,2048]{1,0:T(8,128)(2,1)S(1)}, bf16[48,2048]{1,0:T(8,128)(2,1)S(1)}, u32[]{:S(2)}, u32[]{:S(2)}) %collective-permute-start.13) | collective-permute-done | bytes 196640 | tf_op jit(solution)/shard_map/ppermute | solution.py:27
  143.9 9.3 %collective-permute-done.14 = bf16[48,2048]{1,0:T(8,128)(2,1)S(1)} collective-permute-done((bf16[48,2048]{1,0:T(8,128)(2,1)S(1)}, bf16[48,2048]{1,0:T(8,128)(2,1)S(1)}, u32[]{:S(2)}, u32[]{:S(2)}) %collective-permute-start.14) | collective-permute-done | bytes 196640 | tf_op jit(solution)/shard_map/ppermute | solution.py:27
  154.9 3.8 %fusion.10 = f32[704,768]{1,0:T(8,128)} fusion(f32[704,2048]{1,0:T(8,128)S(1)} %copy-done.4, f32[2048]{0:T(1024)S(1)} %copy-done.5, bf16[1536,2048]{1,0:T(8,128)(2,1)S(1)} %constant_dynamic-update-slice_fusion, s32[]{:T(128)S(6)} %select_n.14), kind=kOutput, calls=%fused_computation.11 | convolution fusion | flops 2220752896 | bytes 11083780 | tf_op jit(solution)/shard_map/dot_general | solution.py:36
  160.4 3.8 %fusion.15 = f32[704,768]{1,0:T(8,128)} fusion(f32[704,2048]{1,0:T(8,128)S(1)} %bitcast.5, f32[2048]{0:T(1024)S(1)} %copy-done.5, bf16[1536,2048]{1,0:T(8,128)(2,1)S(1)} %constant_dynamic-update-slice_fusion, s32[]{:T(128)S(6)} %select_n.14), kind=kOutput, calls=%fused_computation.12 | convolution fusion | flops 2220752896 | bytes 11083780 | tf_op jit(solution)/shard_map/dot_general | solution.py:37
  164.4 3.2 fusion.1
  167.6 2.5 psum.29
  170.1 18.7 %all-reduce.3.cloned.1.call-done = (f32[704,768]{1,0:T(8,128)}, f32[704,768]{1,0:T(8,128)}) async-done(((f32[704,768]{1,0:T(8,128)}, f32[704,768]{1,0:T(8,128)}), (f32[704,768]{1,0:T(8,128)}, f32[704,768]{1,0:T(8,128)})) %all-reduce.3.cloned.1.call-update) | async-done | bytes 4325392 | tf_op jit(solution)/shard_map/psum | solution.py:38
  188.7 9.5 %fusion.2 = f32[768,2048]{1,0:T(8,128)} fusion(f32[704,2048]{1,0:T(8,128)} %param.15, f32[704,768]{1,0:T(8,128)} %get-tuple-element.5, f32[704,768]{1,0:T(8,128)} %get-tuple-element.6, f32[704]{0:T(1024)S(1)} %copy-done.6, f32[704]{0:T(1024)S(1)} %copy-done.7, f32[768]{0:T(1024)S(1)} %add_rsqrt_fusion), kind=kOutput, calls=%fused_computation.4 | convolution fusion | flops 2221441024 | bytes 16392704 | tf_op jit(solution)/shard_map/dot_general | solution.py:44
  198.3 148.2 %reduce-scatter.2.cloned.1.call-done = f32[48,2048]{1,0:T(8,128)} async-done(((f32[768,2048]{1,0:T(8,128)}), f32[48,2048]{1,0:T(8,128)}) %reduce-scatter.2.cloned.1.call-update) | async-done | bytes 393232 | tf_op jit(solution)/shard_map/reduce_scatter | solution.py:43
  347.6 2.5 psum.31
  (75 shorter events, 6.3 us)
Async XLA Ops:
  6.5 148.2 %copy-start = (bf16[48,2048]{1,0:T(8,128)(2,1)S(1)}, bf16[48,2048]{1,0:T(8,128)(2,1)}, u32[]{:S(2)}) copy-start(bf16[48,2048]{1,0:T(8,128)(2,1)} %param.9) | copy-start | bytes 589828
  6.5 182.2 %all-reduce.3.cloned.1.call-start = ((), (), s32[]{:S(2)}) async-start(), calls=%async_computation.2 | async-start | bytes 8650752 | tf_op jit(solution)/shard_map/psum | solution.py:38
  6.5 12.1 %collective-permute-start = (bf16[48,2048]{1,0:T(8,128)(2,1)}, bf16[48,2048]{1,0:T(8,128)(2,1)S(1)}, u32[]{:S(2)}, u32[]{:S(2)}) collective-permute-start(bf16[48,2048]{1,0:T(8,128)(2,1)} %param.9), channel_id=1, source_target_pairs={{0,2},{2,4},{4,6},{6,8},{8,10},{10,12},{12,14},{14,16},{16,18},{18... | collective-permute-start | bytes 589832 | tf_op jit(solution)/shard_map/ppermute | solution.py:27
  18.7 9.7 %collective-permute-start.1 = (bf16[48,2048]{1,0:T(8,128)(2,1)S(1)}, bf16[48,2048]{1,0:T(8,128)(2,1)S(1)}, u32[]{:S(2)}, u32[]{:S(2)}) collective-permute-start(bf16[48,2048]{1,0:T(8,128)(2,1)S(1)} %collective-permute-done), channel_id=1, source_target_pairs={{0,2},{2,4},{4,6},{6,8},{8,10},{10,12},{12,14},{14,16},{16,18},{18... | collective-permute-start | bytes 589832 | tf_op jit(solution)/shard_map/ppermute | solution.py:27
  28.3 9.3 %collective-permute-start.2 = (bf16[48,2048]{1,0:T(8,128)(2,1)S(1)}, bf16[48,2048]{1,0:T(8,128)(2,1)S(1)}, u32[]{:S(2)}, u32[]{:S(2)}) collective-permute-start(bf16[48,2048]{1,0:T(8,128)(2,1)S(1)} %collective-permute-done.1), channel_id=1, source_target_pairs={{0,2},{2,4},{4,6},{6,8},{8,10},{10,12},{12,14},{14,16},{16,18},{18... | collective-permute-start | bytes 589832 | tf_op jit(solution)/shard_map/ppermute | solution.py:27
  37.6 9.3 %collective-permute-start.3 = (bf16[48,2048]{1,0:T(8,128)(2,1)S(1)}, bf16[48,2048]{1,0:T(8,128)(2,1)S(1)}, u32[]{:S(2)}, u32[]{:S(2)}) collective-permute-start(bf16[48,2048]{1,0:T(8,128)(2,1)S(1)} %collective-permute-done.2), channel_id=1, source_target_pairs={{0,2},{2,4},{4,6},{6,8},{8,10},{10,12},{12,14},{14,16},{16,18},{18... | collective-permute-start | bytes 589832 | tf_op jit(solution)/shard_map/ppermute | solution.py:27
  46.9 9.3 %collective-permute-start.4 = (bf16[48,2048]{1,0:T(8,128)(2,1)S(1)}, bf16[48,2048]{1,0:T(8,128)(2,1)S(1)}, u32[]{:S(2)}, u32[]{:S(2)}) collective-permute-start(bf16[48,2048]{1,0:T(8,128)(2,1)S(1)} %collective-permute-done.3), channel_id=1, source_target_pairs={{0,2},{2,4},{4,6},{6,8},{8,10},{10,12},{12,14},{14,16},{16,18},{18... | collective-permute-start | bytes 589832 | tf_op jit(solution)/shard_map/ppermute | solution.py:27
  56.1 9.3 %collective-permute-start.5 = (bf16[48,2048]{1,0:T(8,128)(2,1)S(1)}, bf16[48,2048]{1,0:T(8,128)(2,1)S(1)}, u32[]{:S(2)}, u32[]{:S(2)}) collective-permute-start(bf16[48,2048]{1,0:T(8,128)(2,1)S(1)} %collective-permute-done.4), channel_id=1, source_target_pairs={{0,2},{2,4},{4,6},{6,8},{8,10},{10,12},{12,14},{14,16},{16,18},{18... | collective-permute-start | bytes 589832 | tf_op jit(solution)/shard_map/ppermute | solution.py:27
  65.4 10.4 %collective-permute-start.6 = (bf16[48,2048]{1,0:T(8,128)(2,1)S(1)}, bf16[48,2048]{1,0:T(8,128)(2,1)S(1)}, u32[]{:S(2)}, u32[]{:S(2)}) collective-permute-start(bf16[48,2048]{1,0:T(8,128)(2,1)S(1)} %collective-permute-done.5), channel_id=1, source_target_pairs={{0,2},{2,4},{4,6},{6,8},{8,10},{10,12},{12,14},{14,16},{16,18},{18... | collective-permute-start | bytes 589832 | tf_op jit(solution)/shard_map/ppermute | solution.py:27
  75.8 11.2 %collective-permute-start.7 = (bf16[48,2048]{1,0:T(8,128)(2,1)S(1)}, bf16[48,2048]{1,0:T(8,128)(2,1)S(1)}, u32[]{:S(2)}, u32[]{:S(2)}) collective-permute-start(bf16[48,2048]{1,0:T(8,128)(2,1)S(1)} %collective-permute-done.6), channel_id=1, source_target_pairs={{0,2},{2,4},{4,6},{6,8},{8,10},{10,12},{12,14},{14,16},{16,18},{18... | collective-permute-start | bytes 589832 | tf_op jit(solution)/shard_map/ppermute | solution.py:27
  87.0 10.3 %collective-permute-start.8 = (bf16[48,2048]{1,0:T(8,128)(2,1)S(1)}, bf16[48,2048]{1,0:T(8,128)(2,1)S(1)}, u32[]{:S(2)}, u32[]{:S(2)}) collective-permute-start(bf16[48,2048]{1,0:T(8,128)(2,1)S(1)} %collective-permute-done.7), channel_id=1, source_target_pairs={{0,2},{2,4},{4,6},{6,8},{8,10},{10,12},{12,14},{14,16},{16,18},{18... | collective-permute-start | bytes 589832 | tf_op jit(solution)/shard_map/ppermute | solution.py:27
  97.3 9.5 %collective-permute-start.9 = (bf16[48,2048]{1,0:T(8,128)(2,1)S(1)}, bf16[48,2048]{1,0:T(8,128)(2,1)S(1)}, u32[]{:S(2)}, u32[]{:S(2)}) collective-permute-start(bf16[48,2048]{1,0:T(8,128)(2,1)S(1)} %collective-permute-done.8), channel_id=1, source_target_pairs={{0,2},{2,4},{4,6},{6,8},{8,10},{10,12},{12,14},{14,16},{16,18},{18... | collective-permute-start | bytes 589832 | tf_op jit(solution)/shard_map/ppermute | solution.py:27
  106.8 9.3 %collective-permute-start.10 = (bf16[48,2048]{1,0:T(8,128)(2,1)S(1)}, bf16[48,2048]{1,0:T(8,128)(2,1)S(1)}, u32[]{:S(2)}, u32[]{:S(2)}) collective-permute-start(bf16[48,2048]{1,0:T(8,128)(2,1)S(1)} %collective-permute-done.9), channel_id=1, source_target_pairs={{0,2},{2,4},{4,6},{6,8},{8,10},{10,12},{12,14},{14,16},{16,18},{18... | collective-permute-start | bytes 589832 | tf_op jit(solution)/shard_map/ppermute | solution.py:27
  116.1 9.3 %collective-permute-start.11 = (bf16[48,2048]{1,0:T(8,128)(2,1)S(1)}, bf16[48,2048]{1,0:T(8,128)(2,1)S(1)}, u32[]{:S(2)}, u32[]{:S(2)}) collective-permute-start(bf16[48,2048]{1,0:T(8,128)(2,1)S(1)} %collective-permute-done.10), channel_id=1, source_target_pairs={{0,2},{2,4},{4,6},{6,8},{8,10},{10,12},{12,14},{14,16},{16,18},{18... | collective-permute-start | bytes 589832 | tf_op jit(solution)/shard_map/ppermute | solution.py:27
  125.3 9.3 %collective-permute-start.12 = (bf16[48,2048]{1,0:T(8,128)(2,1)S(1)}, bf16[48,2048]{1,0:T(8,128)(2,1)S(1)}, u32[]{:S(2)}, u32[]{:S(2)}) collective-permute-start(bf16[48,2048]{1,0:T(8,128)(2,1)S(1)} %collective-permute-done.11), channel_id=1, source_target_pairs={{0,2},{2,4},{4,6},{6,8},{8,10},{10,12},{12,14},{14,16},{16,18},{18... | collective-permute-start | bytes 589832 | tf_op jit(solution)/shard_map/ppermute | solution.py:27
  134.6 9.3 %collective-permute-start.13 = (bf16[48,2048]{1,0:T(8,128)(2,1)S(1)}, bf16[48,2048]{1,0:T(8,128)(2,1)S(1)}, u32[]{:S(2)}, u32[]{:S(2)}) collective-permute-start(bf16[48,2048]{1,0:T(8,128)(2,1)S(1)} %collective-permute-done.12), channel_id=1, source_target_pairs={{0,2},{2,4},{4,6},{6,8},{8,10},{10,12},{12,14},{14,16},{16,18},{18... | collective-permute-start | bytes 589832 | tf_op jit(solution)/shard_map/ppermute | solution.py:27
  143.9 9.3 %collective-permute-start.14 = (bf16[48,2048]{1,0:T(8,128)(2,1)S(1)}, bf16[48,2048]{1,0:T(8,128)(2,1)S(1)}, u32[]{:S(2)}, u32[]{:S(2)}) collective-permute-start(bf16[48,2048]{1,0:T(8,128)(2,1)S(1)} %collective-permute-done.13), channel_id=1, source_target_pairs={{0,2},{2,4},{4,6},{6,8},{8,10},{10,12},{12,14},{14,16},{16,18},{18... | collective-permute-start | bytes 589832 | tf_op jit(solution)/shard_map/ppermute | solution.py:27
  143.9 10.9 %copy-start.4 = (f32[704,2048]{1,0:T(8,128)S(1)}, f32[704,2048]{1,0:T(8,128)}, u32[]{:S(2)}) copy-start(f32[704,2048]{1,0:T(8,128)} %param.11) | copy-start | bytes 17301508
  143.9 11.0 %copy-start.5 = (f32[2048]{0:T(1024)S(1)}, f32[2048]{0:T(1024)}, u32[]{:S(2)}) copy-start(f32[2048]{0:T(1024)} %param.10) | copy-start | bytes 24580
  164.3 24.5 %copy-start.6 = (f32[704]{0:T(1024)S(1)}, f32[704]{0:T(1024)}, u32[]{:S(2)}) copy-start(f32[704]{0:T(1024)} %param.14) | copy-start | bytes 8452
  164.3 24.5 %copy-start.7 = (f32[704]{0:T(1024)S(1)}, f32[704]{0:T(1024)}, u32[]{:S(2)}) copy-start(f32[704]{0:T(1024)} %param.12) | copy-start | bytes 8452
  164.3 182.1 %reduce-scatter.2.cloned.1.call-start = ((), (), s32[]{:S(2)}) async-start(), calls=%async_computation.1 | async-start | bytes 6684672 | tf_op jit(solution)/shard_map/reduce_scatter | solution.py:43
  198.2 148.2 %copy-start.2 = (f32[2048]{0:T(1024)S(1)}, f32[2048]{0:T(1024)}, u32[]{:S(2)}) copy-start(f32[2048]{0:T(1024)} %param.16) | copy-start | bytes 24580
  198.2 151.8 %copy-start.3 = (f32[2048]{0:T(1024)S(1)}, f32[2048]{0:T(1024)}, u32[]{:S(2)}) copy-start(f32[2048]{0:T(1024)} %param.17) | copy-start | bytes 24580
  (3 other events, 15.0 us)
Sparse Core Ops, SparseCore 0:
  164.4 24.2 all-reduce.2
  198.4 147.9 reduce-scatter.1
